TPU v7x, 512 devices: a whole 4x4x16 slice. The times are simulated.
512 devices in a mesh: sp: 16 (over z), fs: 4 (over y), tp: 8 (over x, core).
Axes of the slice: x: 4, y: 4, z: 16, core: 2. Of those that a mesh axis runs over, the one named last changes fastest.
Arguments:
- tokens: bfloat16 [16384, 2048], P(('fs', 'sp', 'tp')), parts along dimension 0, may hold values from -6 to 6
- norm_gain: bfloat16 [2048], replicated, may hold values from 0.099609375 to 1.8984375
- w_pool_in: bfloat16 [2048, 1024], P('sp', 'tp'), may hold values from -0.125 to 0.125
- w_query: bfloat16 [2048, 1024], P('sp', 'tp'), may hold values from -0.125 to 0.125
- w_key: bfloat16 [2048, 1024], P('sp', 'tp'), may hold values from -0.125 to 0.125
- w_value: bfloat16 [2048, 1024], P('sp', 'tp'), may hold values from -0.125 to 0.125
- w_gate: bfloat16 [2048, 1024], P('sp', 'tp'), may hold values from -0.125 to 0.125
- w_beta: bfloat16 [2048, 8], replicated, may hold values from -0.125 to 0.125
- w_decay: bfloat16 [2048, 8], replicated, may hold values from -0.5 to 0.5
- conv_weight: float32 [3, 4, 1024], P(None, None, 'tp'), may hold values from -3 to 3
- a_log: float32 [8], P('tp'), may hold values from -20 to -1.7, as said below
- decay_extra: float32 [16384, 8], P(('fs', 'sp'), 'tp'), parts along dimension 0, may hold values from -1.4 to 0
- w_mix: bfloat16 [8, 128, 128], P('tp'), may hold values from -0.5 to 0.5
- pool_scale: float32 [1024], P('tp'), may hold values from 0.1 to 1.9
- delta_gain: float32 [128], replicated, may hold values from 0.1 to 1.9
- w_out_pool: bfloat16 [1024, 2048], P('tp', 'sp'), may hold values from -0.125 to 0.125
- w_out_delta: bfloat16 [1024, 2048], P('tp', 'sp'), may hold values from -0.125 to 0.125
Outputs:
- mixed: bfloat16 [16384, 2048], P(('fs', 'sp', 'tp')), parts along dimension 0
There are 4 independent parts, one for each index of `fs`. A program takes and returns all parts, laid end to end along the dimension named above; an argument that names none is the same for every part. Nothing has to cross between parts.
Inputs may be any that keep to these rules, and one draw needn't show every extreme that they name: `a_log`: logarithm of each head's base decay rate.
All inputs are finite; a program needn't handle non-finite values.
Results may differ from a plain program's by a relative error of at most 0.018.
Values may be sent and summed in bfloat16 or wider, within the bound.
No kernel may reach another device: no remote copies, remote signals or barrier semaphores. Data moves between devices by JAX's collectives and lax.ppermute only.
A program may use at most 64 MiB of HBM per device.

v0:
```python
import jax
import jax.numpy as jnp
from jax import lax
from jax.sharding import PartitionSpec as P

BLOCK = 64
eps = 1e-06
windows = (2, 4, 8, 16)
tail_rows = 15


def turned_gather(arrays, axis, dims):
    turned = [jnp.moveaxis(a, dim, 0) for a, dim in zip(arrays, dims)]
    both = jnp.concatenate([t.reshape(len(t), -1) for t in turned], axis=1)
    out, at, finished = (lax.all_gather(both, axis, axis=0, tiled=True), 0, [])
    for t, dim in zip(turned, dims):
        slab = out[:, at : at + t[0].size].reshape(-1, *t.shape[1:])
        finished.append(jnp.moveaxis(slab, 0, dim))
        at += t[0].size
    return tuple(finished)


def copy_for_each(x, axis):
    copies = jnp.broadcast_to(x, (lax.axis_size(axis), *x.shape))
    return lax.all_to_all(copies, axis, split_axis=0, concat_axis=0, tiled=True)


def laid_out(blocks, dim):
    lengths = list(blocks.shape[1:])
    lengths[dim] *= blocks.shape[0]
    return jnp.moveaxis(blocks, 0, dim).reshape(lengths)


def gather_directly(x, axis, dim):
    blocks = copy_for_each(x, axis)
    return laid_out(blocks, dim)


def from_behind(block, axis, distance):
    devices = range(lax.axis_size(axis))
    route = [(i - distance, i) for i in devices if i - distance in devices]
    return lax.ppermute(block, axis, route)


def entering(x, axis, join, neutral):
    place = lax.axis_index(axis)
    gathered = jax.tree.map(
        lambda a, kind: lax.all_gather(a.astype(kind), axis), x, (jnp.bfloat16, jnp.bfloat16)
    )
    state = jax.tree.map(lambda a, e: jnp.zeros_like(a) + jnp.asarray(e, a.dtype), x, neutral)

    def one(hop, state):
        return join(
            state,
            jax.tree.map(
                lambda a, own: lax.dynamic_index_in_dim(a, hop, 0, False).astype(own.dtype),
                gathered,
                x,
            ),
        )

    return lax.fori_loop(0, place, one, state)


def side_by_side(arrays, axis, dim, along):
    ends, at = ([], 0)
    for a in arrays[:-1]:
        at += a.shape[along]
        ends.append(at)
    both = jnp.concatenate(arrays, axis=along)
    return tuple(jnp.split(lax.all_gather(both, axis, axis=dim, tiled=True), ends, axis=along))


def rms_rows(values, gain):
    floats = values.astype(jnp.float32)
    scale = lax.rsqrt(jnp.mean(floats * floats, axis=-1, keepdims=True) + eps)
    return (floats * scale * gain.astype(jnp.float32)).astype(jnp.bfloat16)


def unit_rows(values):
    return values * lax.rsqrt(jnp.sum(values * values, axis=-1, keepdims=True) + eps)


def block_terms(query, keys, values, log_gate, strength, block):
    heads, length, width = keys.shape
    count = length // block

    def split(tensor):
        return tensor.reshape(heads, count, block, tensor.shape[-1])

    query_part, key_part, value_part = (split(query), split(keys), split(values))
    gate_cum = jnp.cumsum(log_gate.reshape(heads, count, block), axis=-1)
    beta_part = strength.reshape(heads, count, block)[..., None]
    lower_mask = jnp.tril(jnp.ones((block, block), dtype=bool))
    strict_mask = jnp.tril(jnp.ones((block, block), dtype=bool), k=-1)
    gaps = gate_cum[..., :, None] - gate_cum[..., None, :]
    decay_tab = jnp.where(lower_mask, jnp.exp(jnp.where(lower_mask, gaps, 0.0)), 0.0)
    key_scaled_beta = key_part * beta_part
    value_beta = value_part * beta_part
    corr_lower = jnp.where(
        strict_mask, jnp.einsum("hnid,hnjd->hnij", key_scaled_beta, key_part) * decay_tab, 0.0
    )
    identity = jnp.eye(block, dtype=jnp.float32)
    inverse = lax.linalg.triangular_solve(
        identity + corr_lower,
        jnp.broadcast_to(identity, corr_lower.shape),
        left_side=True,
        lower=True,
    )
    fixed_values = jnp.einsum("hnij,hnjd->hnid", inverse, value_beta)
    key_weights = jnp.einsum(
        "hnij,hnjd->hnid", inverse, key_scaled_beta * jnp.exp(gate_cum)[..., None]
    )
    scores = jnp.where(
        lower_mask, jnp.einsum("hnid,hnjd->hnij", query_part, key_part) * decay_tab, 0.0
    )
    key_decayed = key_part * jnp.exp(gate_cum[..., -1:] - gate_cum)[..., None]
    query_gated = query_part * jnp.exp(gate_cum)[..., None]
    terms = (query_gated, key_decayed, fixed_values, key_weights, scores, gate_cum[..., -1])
    return tuple((jnp.moveaxis(tensor, 1, 0) for tensor in terms))


def carry_step(state, inputs):
    query_gated, key_decayed, fixed_values, key_weights, scores, last_gate = inputs
    fresh = fixed_values - jnp.einsum("hcd,hde->hce", key_weights, state)
    output = jnp.einsum("hcd,hde->hce", query_gated, state) + jnp.einsum(
        "hij,hje->hie", scores, fresh
    )
    state = state * jnp.exp(last_gate)[:, None, None] + jnp.einsum(
        "hcd,hce->hde", key_decayed, fresh
    )
    return (state, output)


def compose_step(carry, inputs):
    linear, offset = carry
    query_gated, key_decayed, fixed_values, key_weights, scores, last_gate = inputs
    fade = jnp.exp(last_gate)[:, None, None]
    moved = jnp.einsum("hcd,hde->hce", key_weights, linear)
    linear = fade * linear - jnp.einsum("hcd,hce->hde", key_decayed, moved)
    fresh = fixed_values - jnp.einsum("hcd,hde->hce", key_weights, offset)
    offset = fade * offset + jnp.einsum("hcd,hce->hde", key_decayed, fresh)
    return ((linear, offset), None)


def apply_map(linear, state):
    return jnp.einsum("hij,hjk->hik", linear, state)


def combine_maps(earlier, later):
    return (apply_map(later[0], earlier[0]), apply_map(later[0], earlier[1]) + later[1])


def per_device(
    tokens,
    norm_gain,
    w_pool_in,
    w_query,
    w_key,
    w_value,
    w_gate,
    w_beta,
    w_decay,
    conv_weight,
    a_log,
    decay_extra,
    w_mix,
    pool_scale,
    delta_gain,
    w_out_pool,
    w_out_delta,
):
    pool_w, query_w, key_w, value_w, gate_w, outp_w, outd_w = turned_gather(
        (w_pool_in, w_query, w_key, w_value, w_gate, w_out_pool, w_out_delta),
        "sp",
        (0, 0, 0, 0, 0, 1, 1),
    )
    rows_all = gather_directly(tokens, "tp", 0)
    norm_result = rms_rows(rows_all, norm_gain)
    length = norm_result.shape[0]

    def project(weight):
        return jnp.dot(norm_result, weight, preferred_element_type=jnp.float32).astype(jnp.bfloat16)

    pool_in = project(pool_w)
    query_raw = project(query_w)
    key_raw = project(key_w)
    value_raw = project(value_w)
    gate_raw = project(gate_w)
    heads_dev = a_log.shape[0]
    head_dim = query_raw.shape[1] // heads_dev
    width_dev = heads_dev * head_dim
    all_heads = w_beta.shape[1]
    lane = lax.axis_index("tp")
    both_pre = jnp.dot(
        norm_result, jnp.concatenate([w_beta, w_decay], axis=1), preferred_element_type=jnp.float32
    )
    beta_pre = lax.dynamic_slice_in_dim(both_pre[:, :all_heads], lane * heads_dev, heads_dev, 1)
    forget_logits = lax.dynamic_slice_in_dim(
        both_pre[:, all_heads:], lane * heads_dev, heads_dev, 1
    )
    raw_three = jnp.concatenate([query_raw, key_raw, value_raw], axis=1)
    tails = jnp.concatenate(
        [pool_in[length - tail_rows :], raw_three[length - tail_rows :]], axis=1
    )
    prior_state = from_behind(tails, "sp", 1)
    pool_width_dev = pool_in.shape[1]
    source_rows = pool_in.astype(jnp.float32)
    extended = jnp.concatenate(
        [prior_state[:, :pool_width_dev].astype(jnp.float32), source_rows], axis=0
    )
    running = jnp.concatenate(
        [jnp.zeros((1, pool_width_dev), jnp.float32), jnp.cumsum(extended, axis=0)], axis=0
    )
    groups_dev = w_mix.shape[0]
    group_dim = w_mix.shape[1]
    group = lane * groups_dev + jnp.arange(pool_width_dev) // group_dim
    span = (2 ** (1 + group % 4)).astype(jnp.int32)
    ending = running[tail_rows + 1 : tail_rows + 1 + length]
    window_sum = jnp.zeros((length, pool_width_dev), jnp.float32)
    for width in windows:
        lagged = running[tail_rows + 1 - width : tail_rows + 1 - width + length]
        window_sum = window_sum + jnp.where(span[None, :] == width, ending - lagged, 0.0)
    positions = lax.axis_index("sp") * length + jnp.arange(length)
    counts = jnp.minimum(positions[:, None] + 1, span[None, :]).astype(jnp.float32)
    pooled = (window_sum / counts - source_rows).astype(jnp.bfloat16)
    mixed_pool = jnp.einsum(
        "sgc,gcd->sgd",
        pooled.reshape(length, groups_dev, group_dim),
        w_mix,
        preferred_element_type=jnp.float32,
    )
    pool_out = (mixed_pool.reshape(length, pool_width_dev) * pool_scale).astype(jnp.bfloat16)
    taps = conv_weight.shape[1]
    kernel = jnp.transpose(conv_weight, (1, 0, 2)).reshape(taps, 3 * width_dev)
    stacked = jnp.concatenate(
        [prior_state[tail_rows - (taps - 1) :, pool_width_dev:], raw_three], axis=0
    ).astype(jnp.float32)
    conv = jnp.zeros((length, 3 * width_dev), jnp.float32)
    for tap in range(taps):
        conv = conv + stacked[tap : tap + length] * kernel[tap]
    after_silu = jax.nn.silu(conv)

    def heads_first(tensor):
        return jnp.transpose(tensor.reshape(length, heads_dev, head_dim), (1, 0, 2))

    query = unit_rows(heads_first(after_silu[:, :width_dev])) * head_dim ** (-0.5)
    keys = unit_rows(heads_first(after_silu[:, width_dev : 2 * width_dev]))
    values = heads_first(after_silu[:, 2 * width_dev :])
    strength = jax.nn.sigmoid(beta_pre).T
    log_gate = (-jnp.exp(a_log)[None, :] * jax.nn.softplus(forget_logits) + decay_extra).T
    terms = block_terms(query, keys, values, log_gate, strength, BLOCK)
    identity = jnp.broadcast_to(
        jnp.eye(head_dim, dtype=jnp.float32), (heads_dev, head_dim, head_dim)
    )
    empty = jnp.zeros((heads_dev, head_dim, head_dim), jnp.float32)
    (linear, offset), _ = lax.scan(compose_step, (identity, empty), terms)
    prefix = entering((linear, offset), "sp", combine_maps, (identity, empty))
    incoming = prefix[1]
    _, outputs = lax.scan(carry_step, incoming, terms)
    attended = jnp.transpose(outputs, (1, 0, 2, 3)).reshape(heads_dev, length, head_dim)
    normal_out = (
        attended
        * lax.rsqrt(jnp.mean(attended * attended, axis=-1, keepdims=True) + eps)
        * delta_gain
    )
    gated = normal_out * jax.nn.silu(heads_first(gate_raw.astype(jnp.float32)))
    delta_out = jnp.transpose(gated, (1, 0, 2)).reshape(length, width_dev).astype(jnp.bfloat16)
    groups = lax.axis_size("tp")
    rows = length // groups
    both = jnp.concatenate([pool_out, delta_out], axis=1)
    arrived = lax.all_to_all(both, "tp", split_axis=0, concat_axis=0, tiled=True).reshape(
        groups, rows, pool_width_dev + width_dev
    )
    pool_rows, delta_rows = side_by_side((outp_w, outd_w), "tp", 0, 1)
    part_pool = jnp.einsum(
        "jrp,jpd->jrd",
        arrived[..., :pool_width_dev],
        pool_rows.reshape(groups, pool_width_dev, -1),
        preferred_element_type=jnp.float32,
    )
    part_delta = jnp.einsum(
        "jrp,jpd->jrd",
        arrived[..., pool_width_dev:],
        delta_rows.reshape(groups, width_dev, -1),
        preferred_element_type=jnp.float32,
    )
    value_partial_rows = lax.optimization_barrier(
        (part_pool + part_delta).astype(jnp.bfloat16)
    ).astype(jnp.float32)
    result = jnp.sum(value_partial_rows, axis=0)
    return result.astype(jnp.bfloat16)


def solution(mesh):
    placed = (
        P(("fs", "sp", "tp"), None),
        P(),
        P("sp", "tp"),
        P("sp", "tp"),
        P("sp", "tp"),
        P("sp", "tp"),
        P("sp", "tp"),
        P(),
        P(),
        P(None, None, "tp"),
        P("tp"),
        P(("fs", "sp"), "tp"),
        P("tp", None, None),
        P("tp"),
        P(),
        P("tp", "sp"),
        P("tp", "sp"),
    )
    return jax.shard_map(
        per_device,
        mesh=mesh,
        in_specs=placed,
        out_specs=P(("fs", "sp", "tp"), None),
        check_vma=False,
    )
```

profile of v0, /device:TPU:1, one launch (start us, length us, event | category | flops | bytes accessed | tf_op | source)
XLA Modules:
  0.0 249.7 jit_solution(6866411914422944330)
XLA Ops:
  6.5 0.9 copy.78
  7.4 0.9 copy.79
  8.3 0.9 copy.80
  9.2 0.9 copy.81
  10.1 0.9 copy.82
  11.0 0.8 bitcast_dynamic-update-slice_fusion.1
  11.8 0.8 bitcast_dynamic-update-slice_fusion
  12.5 0.7 copy-done.2
  13.3 2.0 broadcast_in_dim.91
  15.3 10.4 %all-to-all-start = ((bf16[8,32,2048]{2,1,0:T(8,128)(2,1)}), bf16[8,32,2048]{2,1,0:T(8,128)(2,1)S(1)}, u32[]{:S(2)}, u32[]{:S(2)}) async-start(bf16[8,32,2048]{2,1,0:T(8,128)(2,1)} %broadcast_in_dim.91), calls=%async_computation | async-start | bytes 2097152 | tf_op jit(solution)/shard_map/all_to_all | solution.py:25
  26.5 71.0 %all-gather.5.cloned.1.call-done = bf16[2048,896]{0,1:T(8,128)(2,1)} async-done(((bf16[128,896]{0,1:T(8,128)(2,1)}), bf16[2048,896]{0,1:T(8,128)(2,1)}) %all-gather.5.cloned.1.call-update) | async-done | bytes 3670032 | tf_op jit(solution)/shard_map/all_gather | solution.py:15
  97.5 1.3 slice_bitcast_fusion.1
  98.8 1.1 pad_maximum_fusion
  100.1 0.3 multiply_reduce_fusion
  100.5 0.3 fusion.59
  100.8 0.4 fusion.100
  101.4 0.2 reduce_window_sum.30
  101.6 0.2 slice_reduce_fusion
  101.8 1.5 fusion.131
  103.3 1.5 convolution_convert_fusion.1
  104.8 1.5 convolution_convert_fusion.2
  106.3 1.5 convolution_convert_fusion.3
  107.8 3.3 %collective-permute-start = (bf16[15,512]{1,0:T(8,128)(2,1)S(1)}, bf16[15,512]{1,0:T(8,128)(2,1)S(1)}, u32[]{:S(2)}, u32[]{:S(2)}) collective-permute-start(bf16[15,512]{1,0:T(8,128)(2,1)S(1)} %fusion.115), channel_id=1, source_target_pairs={{0,32},{32,64},{64,96},{96,128},{128,160},{160,192},{192,224},{224... | collective-permute-start | bytes 46088 | tf_op jit(solution)/shard_map/ppermute | solution.py:42
  111.2 0.7 collective-permute-done
  112.3 0.2 divide_multiply_fusion
  112.9 0.2 fusion.65
  113.1 19.7 %custom-call.3 = f32[1,4,1,64,64]{3,4,2,1,0:T(8,128)S(1)} custom-call(f32[1,4,1,64,64]{4,3,2,1,0:T(8,128)S(1)} %fusion.65), custom_call_target="InvertDiagBlocksLowerTriangular" | custom-call | tf_op jit(solution)/shard_map/triangular_solve | solution.py:104
  132.8 0.4 fusion.91
  133.2 0.2 convolution_bitcast_fusion.3
  133.4 0.3 convolution_bitcast_fusion.4
  133.8 9.7 %while.39 = (s32[]{:T(128)}, f32[1,128,128]{2,1,0:T(8,128)S(1)}, f32[1,128,128]{2,1,0:T(8,128)S(1)}, f32[4,1]{0,1:T(1,128)S(1)}, bf16[4,1,64,128]{3,2,1,0:T(8,12...) while((s32[]{:T(128)}, f32[1,128,128]{2,1,0:T(8,128)S(1)}, ...), condition=%wide.region_6.7_spmd.clone, body=%wide.region_5.6_spmd.clone.sunk | while | flops 8503299 | bytes 757378 | solution.py:257
  133.8 0.6 fusion.206
  134.5 0.9 fusion.208
  135.4 0.9 fusion.207
  136.3 0.6 fusion.206
  136.9 0.9 fusion.208
  137.8 0.9 fusion.207
  138.7 0.6 fusion.206
  139.3 0.9 fusion.208
  140.2 0.9 fusion.207
  141.1 0.6 fusion.206
  141.7 0.9 fusion.208
  142.6 0.9 fusion.207
  143.5 0.2 fusion.61
  143.8 26.1 %all-gather = bf16[16,128,128]{2,1,0:T(8,128)(2,1)S(1)} all-gather(bf16[1,128,128]{2,1,0:T(8,128)(2,1)S(1)} %convert_element_type.116), channel_id=2, replica_groups=mesh['sp'=16,'fs'=4,'tp'=8] {'sp'}, dimensions={0}, use_global_device_ids=true | all-gather | bytes 557056 | tf_op jit(solution)/shard_map/all_gather | solution.py:48
  169.9 24.1 %all-gather.1 = bf16[16,128,128]{2,1,0:T(8,128)(2,1)S(1)} all-gather(bf16[1,128,128]{2,1,0:T(8,128)(2,1)S(1)} %convert_element_type.117), channel_id=3, replica_groups=mesh['sp'=16,'fs'=4,'tp'=8] {'sp'}, dimensions={0}, use_global_device_ids=true | all-gather | bytes 557056 | tf_op jit(solution)/shard_map/all_gather | solution.py:48
  194.0 7.4 %while.38 = (s32[]{:T(128)}, f32[1,128,128]{2,1,0:T(8,128)S(1)}, f32[4,1,64,128]{3,2,1,0:T(8,128)S(1)}, f32[4,1]{0,1:T(1,128)S(1)}, bf16[4,1,64,128]{3,2,1,0:T(8...) while((s32[]{:T(128)}, f32[1,128,128]{2,1,0:T(8,128)S(1)}, ...), condition=%wide.region_11.12_spmd, body=%wide.region_10.11_spmd.sunk | while | flops 7397378 | bytes 510085 | solution.py:260
  194.0 0.6 fusion.195
  194.9 0.8 fusion.196
  195.9 0.6 fusion.195
  196.8 0.8 fusion.196
  197.7 0.6 fusion.195
  198.6 0.8 fusion.196
  199.6 0.6 fusion.195
  200.4 0.8 fusion.196
  201.6 0.3 fusion.110
  201.9 1.5 fusion.90
  203.4 0.7 pad_maximum_fusion.1
  204.1 27.8 %all-to-all-start.1 = ((bf16[8,32,256]{2,1,0:T(8,128)(2,1)}), bf16[8,32,256]{2,1,0:T(8,128)(2,1)S(1)}, u32[]{:S(2)}, u32[]{:S(2)}) async-start(bf16[8,32,256]{2,1,0:T(8,128)(2,1)} %pad_maximum_fusion.1), calls=%async_computation.1 | async-start | bytes 262144 | tf_op jit(solution)/shard_map/all_to_all | solution.py:272
  231.9 6.0 %fusion.129 = (bf16[1024,2048]{1,0:T(8,128)(2,1)}, bf16[1024,2048]{1,0:T(8,128)(2,1)}) fusion(bf16[1024,4096]{1,0:T(8,128)(2,1)} %all-gather.7.cloned.1.call-done), kind=kLoop, calls=%fused_computation.205 | loop fusion | bytes 16777216 | tf_op jit(solution)/shard_map/split | solution.py:71
  237.9 3.0 %fusion.98 = f32[8,32,2048]{2,1,0:T(8,128)S(1)} fusion(bf16[8,128,2048]{2,1,0:T(8,128)(2,1)} %bitcast.262, bf16[8,32,256]{2,1,0:T(8,128)(2,1)S(1)} %all-to-all-done.1), kind=kOutput, calls=%fused_computation.129 | convolution fusion | flops 134217728 | bytes 6356992 | tf_op jit(solution)/shard_map/jrp,jpd->jrd/dot_general | solution.py:276
  240.9 0.4 copy-done.1
  241.4 0.7 fusion.57
  242.1 0.8 reduce_sum.52
  (95 shorter events, 3.4 us)
Async XLA Ops:
  6.5 195.1 %copy-start = (bf16[1,128,128]{2,1,0:T(8,128)(2,1)S(1)}, bf16[1,128,128]{2,1,0:T(8,128)(2,1)}, u32[]{:S(2)}) copy-start(bf16[1,128,128]{2,1,0:T(8,128)(2,1)} %param.35) | copy-start | bytes 98308
  6.5 19.9 %copy-start.6 = (bf16[2048]{0:T(1024)(128)(2,1)S(1)}, bf16[2048]{0:T(1024)(128)(2,1)}, u32[]{:S(2)}) copy-start(bf16[2048]{0:T(1024)(128)(2,1)} %param.24) | copy-start | bytes 12292
  6.5 90.9 %all-gather.5.cloned.1.call-start = ((), (), s32[]{:S(2)}) async-start(), calls=%async_computation.2 | async-start | bytes 3899392 | tf_op jit(solution)/shard_map/all_gather | solution.py:15
  12.5 0.7 copy-start.2
  15.3 84.7 %copy-start.5 = (f32[3,4,128]{2,1,0:T(4,128)S(1)}, f32[3,4,128]{2,1,0:T(4,128)}, u32[]{:S(2)}) copy-start(f32[3,4,128]{2,1,0:T(4,128)} %param.32) | copy-start | bytes 18436
  15.3 84.9 %all-to-all-start = ((bf16[8,32,2048]{2,1,0:T(8,128)(2,1)}), bf16[8,32,2048]{2,1,0:T(8,128)(2,1)S(1)}, u32[]{:S(2)}, u32[]{:S(2)}) async-start(bf16[8,32,2048]{2,1,0:T(8,128)(2,1)} %broadcast_in_dim.91), calls=%async_computation | async-start | bytes 2097152 | tf_op jit(solution)/shard_map/all_to_all | solution.py:25
  25.7 206.2 %all-gather.7.cloned.1.call-start = ((), (), s32[]{:S(2)}) async-start(), calls=%async_computation.3 | async-start | bytes 9437184 | tf_op jit(solution)/shard_map/all_gather | solution.py:71
  98.8 2.1 copy-start.3
  98.8 2.1 copy-start.4
  98.8 2.4 copy-start.7
  107.8 4.2 %collective-permute-start = (bf16[15,512]{1,0:T(8,128)(2,1)S(1)}, bf16[15,512]{1,0:T(8,128)(2,1)S(1)}, u32[]{:S(2)}, u32[]{:S(2)}) collective-permute-start(bf16[15,512]{1,0:T(8,128)(2,1)S(1)} %fusion.115), channel_id=1, source_target_pairs={{0,32},{32,64},{64,96},{96,128},{128,160},{160,192},{192,224},{224... | collective-permute-start | bytes 46088 | tf_op jit(solution)/shard_map/ppermute | solution.py:42
  169.9 31.9 %copy-start.8 = (f32[128]{0:T(128)S(1)}, f32[128]{0:T(128)}, u32[]{:S(2)}) copy-start(f32[128]{0:T(128)} %param.36) | copy-start | bytes 1540
  169.9 32.0 %copy-start.9 = (f32[128]{0:T(128)S(1)}, f32[128]{0:T(128)}, u32[]{:S(2)}) copy-start(f32[128]{0:T(128)} %param.37) | copy-start | bytes 1540
  204.1 33.9 %all-to-all-start.1 = ((bf16[8,32,256]{2,1,0:T(8,128)(2,1)}), bf16[8,32,256]{2,1,0:T(8,128)(2,1)S(1)}, u32[]{:S(2)}, u32[]{:S(2)}) async-start(bf16[8,32,256]{2,1,0:T(8,128)(2,1)} %pad_maximum_fusion.1), calls=%async_computation.1 | async-start | bytes 262144 | tf_op jit(solution)/shard_map/all_to_all | solution.py:272
  237.9 3.5 %copy-start.1 = (bf16[1024,2048]{1,0:T(8,128)(2,1)S(1)}, bf16[1024,2048]{1,0:T(8,128)(2,1)}, u32[]{:S(2)}) copy-start(bf16[1024,2048]{1,0:T(8,128)(2,1)} %get-tuple-element.294) | copy-start | bytes 12582916
Sparse Core Ops, SparseCore 0:
  13.4 84.0 all-gather.4
  100.0 65.0 all-gather.6
where the time goes:
time: 251 us; the launch traced here: 250 us
  waiting for transfers between devices  71.7 us (29%)
  blocking collectives  50.2 us (20%)
  starting transfers between devices  41.6 us (17%)
  matrix products  24.9 us (10%)
  other arithmetic  24.6 us (10%)
  local copies, waits for them, and re-layouts  22.1 us (9%)
  between operations  14.5 us (6%)
    all_gather x1, waiting for transfers between devices, turned_gather(): out, at, finished = (lax.all_gather(both, axis, axis=0, tiled=True), 0, [])  71 us
    all_gather x2, blocking collectives, entering(): lax.all_gather(a.astype(kind), axis)  50.2 us
    all_to_all x1, starting transfers between devices, per_device(): lax.all_to_all(both, 'tp', split_axis=0, concat_axis=0, tiled=True)  27.8 us
    another operation x1, other arithmetic, block_terms(): lax.linalg.triangular_solve(identity + corr_lower, jnp.broadcast_to(ident...  19.7 us
    all_to_all x1, starting transfers between devices, copy_for_each(): return lax.all_to_all(copies, axis, split_axis=0, concat_axis=0, tiled=True)  10.4 us
    dot_general x5, matrix products, project(): jnp.dot(norm_result, weight, preferred_element_type=jnp.float32)  7.41 us
    unnamed x31, local copies, waits for them, and re-layouts  6.34 us
    split x1, local copies, waits for them, and re-layouts, side_by_side(): jnp.split(lax.all_gather(both, axis, axis=dim, tiled=True), ends, axis=al...  6.02 us
  transfers between devices with their start and end apart: 5, of which 2 were waited for; matrix products, arithmetic and copies ran while one was open for 24% of the time, Pallas kernels for 0%

commit v1 on v0

--- a/solution.py
+++ b/solution.py
@@ -9,10 +9,17 @@
 tail_rows = 15
 
 
+def exchange_gather(block, mesh_axis, along):
+    n_dev = lax.axis_size(mesh_axis)
+    blocks = jnp.stack([block for _ in range(n_dev)])
+    blocks = lax.all_to_all(blocks, mesh_axis, split_axis=0, concat_axis=0)
+    return jnp.concatenate(blocks, axis=along)
+
+
 def turned_gather(arrays, axis, dims):
     turned = [jnp.moveaxis(a, dim, 0) for a, dim in zip(arrays, dims)]
     both = jnp.concatenate([t.reshape(len(t), -1) for t in turned], axis=1)
-    out, at, finished = (lax.all_gather(both, axis, axis=0, tiled=True), 0, [])
+    out, at, finished = (exchange_gather(both, axis, 0), 0, [])
     for t, dim in zip(turned, dims):
         slab = out[:, at : at + t[0].size].reshape(-1, *t.shape[1:])
         finished.append(jnp.moveaxis(slab, 0, dim))

time: 251 us -> 367 us (1.46)
  waiting for transfers between devices: 71.7 us -> 166 us
  local copies, waits for them, and re-layouts: 22.1 us -> 42 us
    all_to_all x0 -> x1, waiting for transfers between devices: none -> 159 us  [exchange_gather(): blocks = lax.all_to_all(blocks, mesh_axis, split_axis=0, concat_axis=0)]
    all_gather x1 -> x0, waiting for transfers between devices: 71 us -> none  [turned_gather(): out, at, finished = (lax.all_gather(both, axis, axis=0, tiled=True), 0, [])]
    all_to_all x0 -> x1, starting transfers between devices: none -> 15.9 us  [exchange_gather(): blocks = lax.all_to_all(blocks, mesh_axis, split_axis=0, concat_axis=0)]
    split x1 -> x3, local copies, waits for them, and re-layouts: 6.02 us -> 18.9 us  [side_by_side(): jnp.split(lax.all_gather(both, axis, axis=dim, tiled=True), ends, axis=al...]
    all_to_all x1, starting transfers between devices: 27.8 us -> 18.5 us  [per_device(): lax.all_to_all(both, 'tp', split_axis=0, concat_axis=0, tiled=True)]
    all_to_all x1, waiting for transfers between devices: 0.01 us -> 6.28 us  [copy_for_each(): return lax.all_to_all(copies, axis, split_axis=0, concat_axis=0, tiled=True)]
    all_to_all x0 -> x1, local copies, waits for them, and re-layouts: none -> 6.05 us  [exchange_gather(): blocks = lax.all_to_all(blocks, mesh_axis, split_axis=0, concat_axis=0)]
    all_to_all x1, starting transfers between devices: 10.4 us -> 5.69 us  [copy_for_each(): return lax.all_to_all(copies, axis, split_axis=0, concat_axis=0, tiled=True)]
  transfers between devices with their start and end apart: 5 -> 5, of which waited for: 2 -> 3; matrix products, arithmetic and copies ran while one was open for 24% -> 21% of each run, Pallas kernels for 0% -> 0%
where the time goes in v1:
time: 367 us; the launch traced here: 366 us
  waiting for transfers between devices  166 us (45%)
  blocking collectives  49.7 us (14%)
  starting transfers between devices  44.3 us (12%)
  local copies, waits for them, and re-layouts  42 us (11%)
  matrix products  24.8 us (7%)
  other arithmetic  24.6 us (7%)
  between operations  14.5 us (4%)
    all_to_all x1, waiting for transfers between devices, exchange_gather(): blocks = lax.all_to_all(blocks, mesh_axis, split_axis=0, concat_axis=0)  159 us
    all_gather x2, blocking collectives, entering(): lax.all_gather(a.astype(kind), axis)  49.7 us
    another operation x1, other arithmetic, block_terms(): lax.linalg.triangular_solve(identity + corr_lower, jnp.broadcast_to(ident...  19.7 us
    split x3, local copies, waits for them, and re-layouts, side_by_side(): jnp.split(lax.all_gather(both, axis, axis=dim, tiled=True), ends, axis=al...  18.9 us
    all_to_all x1, starting transfers between devices, per_device(): lax.all_to_all(both, 'tp', split_axis=0, concat_axis=0, tiled=True)  18.5 us
    all_to_all x1, starting transfers between devices, exchange_gather(): blocks = lax.all_to_all(blocks, mesh_axis, split_axis=0, concat_axis=0)  15.9 us
    dot_general x5, matrix products, project(): jnp.dot(norm_result, weight, preferred_element_type=jnp.float32)  7.35 us
  transfers between devices with their start and end apart: 5, of which 3 were waited for; matrix products, arithmetic and copies ran while one was open for 21% of the time, Pallas kernels for 0%

profile of v1, /device:TPU:1, one launch (start us, length us, event | category | flops | bytes accessed | tf_op | source)
XLA Modules:
  0.0 365.7 jit_solution(1280896706267465372)
XLA Ops:
  6.5 0.9 copy.101
  7.4 0.9 copy.102
  8.3 0.9 copy.103
  9.2 0.9 copy.104
  10.0 0.9 copy.105
  11.0 0.8 bitcast_dynamic-update-slice_fusion.1
  11.8 0.8 bitcast_dynamic-update-slice_fusion
  12.5 2.5 stack.2
  15.1 15.9 %all-to-all-start.1 = ((bf16[16,128,896]{1,2,0:T(8,128)(2,1)}), bf16[16,128,896]{1,2,0:T(8,128)(2,1)}, u32[]{:S(2)}, u32[]{:S(2)}) async-start(bf16[16,128,896]{1,2,0:T(8,128)(2,1)} %stack.2), calls=%async_computation.1 | async-start | bytes 7340032 | tf_op jit(solution)/shard_map/all_to_all | solution.py:15
  31.8 158.6 %all-to-all-done.1 = bf16[16,128,896]{1,2,0:T(8,128)(2,1)} async-done(((bf16[16,128,896]{1,2,0:T(8,128)(2,1)}), bf16[16,128,896]{1,2,0:T(8,128)(2,1)}, u32[]{:S(2)}, u32[]{:S(2)}) %all-to-all-start.1) | async-done | bytes 3670048 | tf_op jit(solution)/shard_map/all_to_all | solution.py:15
  190.4 1.1 broadcast_in_dim.91
  191.5 5.7 %all-to-all-start = ((bf16[8,32,2048]{2,1,0:T(8,128)(2,1)}), bf16[8,32,2048]{2,1,0:T(8,128)(2,1)S(1)}, u32[]{:S(2)}, u32[]{:S(2)}) async-start(bf16[8,32,2048]{2,1,0:T(8,128)(2,1)} %broadcast_in_dim.91), calls=%async_computation | async-start | bytes 2097152 | tf_op jit(solution)/shard_map/all_to_all | solution.py:32
  197.2 6.0 %copy.106 = bf16[16,128,896]{2,1,0:T(8,128)(2,1)} copy(bf16[16,128,896]{1,2,0:T(8,128)(2,1)} %all-to-all-done.1) | data formatting | bytes 7340032 | tf_op jit(solution)/shard_map/all_to_all | solution.py:15
  203.3 1.3 slice_bitcast_fusion.1
  204.6 1.1 pad_maximum_fusion
  205.9 6.3 %all-to-all-done = bf16[8,32,2048]{2,1,0:T(8,128)(2,1)S(1)} async-done(((bf16[8,32,2048]{2,1,0:T(8,128)(2,1)}), bf16[8,32,2048]{2,1,0:T(8,128)(2,1)S(1)}, u32[]{:S(2)}, u32[]{:S(2)}) %all-to-all-start) | async-done | bytes 1048608 | tf_op jit(solution)/shard_map/all_to_all | solution.py:32
  212.2 0.3 multiply_reduce_fusion
  212.6 0.3 fusion.59
  212.9 0.4 fusion.100
  213.9 1.5 fusion.131
  215.4 1.5 convolution_convert_fusion.1
  216.8 1.5 convolution_convert_fusion.2
  218.3 1.5 convolution_convert_fusion.3
  219.8 4.2 %collective-permute-start = (bf16[15,512]{1,0:T(8,128)(2,1)S(1)}, bf16[15,512]{1,0:T(8,128)(2,1)S(1)}, u32[]{:S(2)}, u32[]{:S(2)}) collective-permute-start(bf16[15,512]{1,0:T(8,128)(2,1)S(1)} %fusion.115), channel_id=1, source_target_pairs={{0,32},{32,64},{64,96},{96,128},{128,160},{160,192},{192,224},{224... | collective-permute-start | bytes 46088 | tf_op jit(solution)/shard_map/ppermute | solution.py:49
  224.2 0.7 collective-permute-done
  225.3 0.2 divide_multiply_fusion
  226.1 19.7 %custom-call.3 = f32[1,4,1,64,64]{3,4,2,1,0:T(8,128)S(1)} custom-call(f32[1,4,1,64,64]{4,3,2,1,0:T(8,128)S(1)} %fusion.65), custom_call_target="InvertDiagBlocksLowerTriangular" | custom-call | tf_op jit(solution)/shard_map/triangular_solve | solution.py:111
  245.7 0.4 fusion.91
  246.3 0.3 convolution_bitcast_fusion.4
  246.7 9.7 %while.39 = (s32[]{:T(128)}, f32[1,128,128]{2,1,0:T(8,128)S(1)}, f32[1,128,128]{2,1,0:T(8,128)S(1)}, f32[4,1]{0,1:T(1,128)S(1)}, bf16[4,1,64,128]{3,2,1,0:T(8,12...) while((s32[]{:T(128)}, f32[1,128,128]{2,1,0:T(8,128)S(1)}, ...), condition=%wide.region_6.7_spmd.clone, body=%wide.region_5.6_spmd.clone.sunk | while | flops 8503299 | bytes 757378 | solution.py:264
  246.8 0.6 fusion.206
  247.4 0.9 fusion.208
  248.3 0.9 fusion.207
  249.2 0.6 fusion.206
  249.8 0.9 fusion.208
  250.7 0.9 fusion.207
  251.6 0.6 fusion.206
  252.2 0.9 fusion.208
  253.1 0.9 fusion.207
  254.0 0.6 fusion.206
  254.7 0.9 fusion.208
  255.6 0.9 fusion.207
  256.8 26.6 %all-gather = bf16[16,128,128]{2,1,0:T(8,128)(2,1)S(1)} all-gather(bf16[1,128,128]{2,1,0:T(8,128)(2,1)S(1)} %convert_element_type.116), channel_id=2, replica_groups=mesh['sp'=16,'fs'=4,'tp'=8] {'sp'}, dimensions={0}, use_global_device_ids=true | all-gather | bytes 557056 | tf_op jit(solution)/shard_map/all_gather | solution.py:55
  283.4 23.1 %all-gather.1 = bf16[16,128,128]{2,1,0:T(8,128)(2,1)S(1)} all-gather(bf16[1,128,128]{2,1,0:T(8,128)(2,1)S(1)} %convert_element_type.117), channel_id=3, replica_groups=mesh['sp'=16,'fs'=4,'tp'=8] {'sp'}, dimensions={0}, use_global_device_ids=true | all-gather | bytes 557056 | tf_op jit(solution)/shard_map/all_gather | solution.py:55
  306.4 7.4 %while.38 = (s32[]{:T(128)}, f32[1,128,128]{2,1,0:T(8,128)S(1)}, f32[4,1,64,128]{3,2,1,0:T(8,128)S(1)}, f32[4,1]{0,1:T(1,128)S(1)}, bf16[4,1,64,128]{3,2,1,0:T(8...) while((s32[]{:T(128)}, f32[1,128,128]{2,1,0:T(8,128)S(1)}, ...), condition=%wide.region_11.12_spmd, body=%wide.region_10.11_spmd.sunk | while | flops 7397378 | bytes 510085 | solution.py:267
  306.4 0.6 fusion.195
  307.3 0.8 fusion.196
  308.3 0.6 fusion.195
  309.2 0.8 fusion.196
  310.1 0.6 fusion.195
  311.0 0.8 fusion.196
  312.0 0.6 fusion.195
  312.8 0.8 fusion.196
  314.0 0.3 fusion.110
  314.3 1.5 fusion.90
  315.8 0.7 pad_maximum_fusion.1
  316.5 18.5 %all-to-all-start.2 = ((bf16[8,32,256]{2,1,0:T(8,128)(2,1)}), bf16[8,32,256]{2,1,0:T(8,128)(2,1)S(1)}, u32[]{:S(2)}, u32[]{:S(2)}) async-start(bf16[8,32,256]{2,1,0:T(8,128)(2,1)} %pad_maximum_fusion.1), calls=%async_computation.2 | async-start | bytes 262144 | tf_op jit(solution)/shard_map/all_to_all | solution.py:279
  334.9 5.9 %fusion.129 = (bf16[1024,2048]{0,1:T(8,128)(2,1)}, bf16[1024,2048]{0,1:T(8,128)(2,1)}) fusion(bf16[1024,4096]{0,1:T(8,128)(2,1)} %all-gather.4.cloned.1.call-done), kind=kLoop, calls=%fused_computation.205 | loop fusion | bytes 16777216 | tf_op jit(solution)/shard_map/split | solution.py:78
  340.9 6.5 %copy.123 = bf16[1024,2048]{1,0:T(8,128)(2,1)} copy(bf16[1024,2048]{0,1:T(8,128)(2,1)} %get-tuple-element.315) | data formatting | bytes 8388608 | tf_op jit(solution)/shard_map/split | solution.py:78
  347.3 6.5 %copy.122 = bf16[1024,2048]{1,0:T(8,128)(2,1)} copy(bf16[1024,2048]{0,1:T(8,128)(2,1)} %get-tuple-element.316) | data formatting | bytes 8388608 | tf_op jit(solution)/shard_map/split | solution.py:78
  353.9 3.0 fusion.98
  356.9 0.4 copy-done.1
  357.3 0.7 fusion.57
  358.0 0.8 reduce_sum.52
  (98 shorter events, 4.4 us)
Async XLA Ops:
  6.5 307.5 %copy-start = (bf16[1,128,128]{2,1,0:T(8,128)(2,1)S(1)}, bf16[1,128,128]{2,1,0:T(8,128)(2,1)}, u32[]{:S(2)}) copy-start(bf16[1,128,128]{2,1,0:T(8,128)(2,1)} %param.35) | copy-start | bytes 98308
  15.1 16.6 %copy-start.6 = (bf16[2048]{0:T(1024)(128)(2,1)S(1)}, bf16[2048]{0:T(1024)(128)(2,1)}, u32[]{:S(2)}) copy-start(bf16[2048]{0:T(1024)(128)(2,1)} %param.24) | copy-start | bytes 12292
  15.1 175.3 %copy-start.2 = (bf16[32,2048]{1,0:T(8,128)(2,1)S(1)}, bf16[32,2048]{1,0:T(8,128)(2,1)}, u32[]{:S(2)}) copy-start(bf16[32,2048]{1,0:T(8,128)(2,1)} %param.23) | copy-start | bytes 393220
  15.1 175.3 %all-to-all-start.1 = ((bf16[16,128,896]{1,2,0:T(8,128)(2,1)}), bf16[16,128,896]{1,2,0:T(8,128)(2,1)}, u32[]{:S(2)}, u32[]{:S(2)}) async-start(bf16[16,128,896]{1,2,0:T(8,128)(2,1)} %stack.2), calls=%async_computation.1 | async-start | bytes 7340032 | tf_op jit(solution)/shard_map/all_to_all | solution.py:15
  191.5 20.7 %all-to-all-start = ((bf16[8,32,2048]{2,1,0:T(8,128)(2,1)}), bf16[8,32,2048]{2,1,0:T(8,128)(2,1)S(1)}, u32[]{:S(2)}, u32[]{:S(2)}) async-start(bf16[8,32,2048]{2,1,0:T(8,128)(2,1)} %broadcast_in_dim.91), calls=%async_computation | async-start | bytes 2097152 | tf_op jit(solution)/shard_map/all_to_all | solution.py:32
  197.2 137.7 %all-gather.4.cloned.1.call-start = ((), (), s32[]{:S(2)}) async-start(), calls=%async_computation.3 | async-start | bytes 9437184 | tf_op jit(solution)/shard_map/all_gather | solution.py:78
  203.3 2.5 copy-start.5
  204.6 8.3 %copy-start.3 = (bf16[2048,8]{0,1:T(8,128)(2,1)S(1)}, bf16[2048,8]{0,1:T(8,128)(2,1)}, u32[]{:S(2)}) copy-start(bf16[2048,8]{0,1:T(8,128)(2,1)} %param.31) | copy-start | bytes 98308
  204.6 8.3 %copy-start.4 = (bf16[2048,8]{0,1:T(8,128)(2,1)S(1)}, bf16[2048,8]{0,1:T(8,128)(2,1)}, u32[]{:S(2)}) copy-start(bf16[2048,8]{0,1:T(8,128)(2,1)} %param.30) | copy-start | bytes 98308
  204.6 8.7 %copy-start.7 = (f32[256,1]{0,1:T(1,128)S(1)}, f32[256,1]{0,1:T(1,128)}, u32[]{:S(2)}) copy-start(f32[256,1]{0,1:T(1,128)} %param.34) | copy-start | bytes 3076
  219.8 5.1 %collective-permute-start = (bf16[15,512]{1,0:T(8,128)(2,1)S(1)}, bf16[15,512]{1,0:T(8,128)(2,1)S(1)}, u32[]{:S(2)}, u32[]{:S(2)}) collective-permute-start(bf16[15,512]{1,0:T(8,128)(2,1)S(1)} %fusion.115), channel_id=1, source_target_pairs={{0,32},{32,64},{64,96},{96,128},{128,160},{160,192},{192,224},{224... | collective-permute-start | bytes 46088 | tf_op jit(solution)/shard_map/ppermute | solution.py:49
  283.4 30.9 %copy-start.8 = (f32[128]{0:T(128)S(1)}, f32[128]{0:T(128)}, u32[]{:S(2)}) copy-start(f32[128]{0:T(128)} %param.36) | copy-start | bytes 1540
  283.4 30.9 %copy-start.9 = (f32[128]{0:T(128)S(1)}, f32[128]{0:T(128)}, u32[]{:S(2)}) copy-start(f32[128]{0:T(128)} %param.37) | copy-start | bytes 1540
  316.5 37.4 %all-to-all-start.2 = ((bf16[8,32,256]{2,1,0:T(8,128)(2,1)}), bf16[8,32,256]{2,1,0:T(8,128)(2,1)S(1)}, u32[]{:S(2)}, u32[]{:S(2)}) async-start(bf16[8,32,256]{2,1,0:T(8,128)(2,1)} %pad_maximum_fusion.1), calls=%async_computation.2 | async-start | bytes 262144 | tf_op jit(solution)/shard_map/all_to_all | solution.py:279
  353.9 3.5 copy-start.1
Sparse Core Ops, SparseCore 0:
  205.8 61.5 all-gather.3
